TPU v7x, 512 devices: a whole 4x4x16 slice. The times are simulated.
512 devices in a mesh: sp: 64 (over z, y), tp: 8 (over x, core).
Axes of the slice: x: 4, y: 4, z: 16, core: 2. Of those that a mesh axis runs over, the one named last changes fastest.
Arguments:
- tokens: bfloat16 [6144, 4, 1024], P(('sp', 'tp')), may hold values from -6 to 6
- in_gain: float32 [1024], replicated, may hold values from 0.1 to 1.9
- w_query: bfloat16 [1024, 1024], P('sp', 'tp'), may hold values from -0.1875 to 0.1875
- w_key: bfloat16 [1024, 1024], P('sp', 'tp'), may hold values from -0.1875 to 0.1875
- w_value: bfloat16 [1024, 1024], P('sp', 'tp'), may hold values from -0.1875 to 0.1875
- w_gate: bfloat16 [1024, 1024], P('sp', 'tp'), may hold values from -0.1875 to 0.1875
- w_beta: bfloat16 [1024, 8], P('sp', 'tp'), may hold values from -0.1875 to 0.1875
- conv_query: bfloat16 [4, 1024], P(None, 'tp'), may hold values from -3 to 3
- conv_key: bfloat16 [4, 1024], P(None, 'tp'), may hold values from -3 to 3
- conv_value: bfloat16 [4, 1024], P(None, 'tp'), may hold values from -3 to 3
- decay_rate: float32 [8], P('tp'), may hold values from 0.1 to 3
- out_gain: float32 [128], replicated, may hold values from 0.1 to 1.9
- w_out: bfloat16 [1024, 1024], P('tp', 'sp'), may hold values from -0.1875 to 0.1875
Outputs:
- mixed: bfloat16 [6144, 4, 1024], P(('sp', 'tp'))
All inputs are finite; a program needn't handle non-finite values.
Results may differ from a plain program's by a relative error of at most 0.02.
Values may be sent and summed in bfloat16 or wider, within the bound.
A program may use at most 64 MiB of HBM per device.

v0:
```python
import math

import jax
import jax.numpy as jnp
from jax import lax
from jax.sharding import Mesh
from jax.sharding import PartitionSpec as P

BLOCK = 32
SP = ("sp_0", "sp_1")
TP = ("tp_0", "tp_1")
SP_TP = ("sp_0", "sp_1", "tp_0", "tp_1")


epsilon = 1e-06
out_epsilon = 1e-10
highest = lax.Precision.DEFAULT


def in_order(pieces, dim):
    pieces = jnp.moveaxis(pieces, 0, dim)
    dims = pieces.shape
    return pieces.reshape(*dims[:dim], dims[dim] * dims[dim + 1], *dims[dim + 2 :])


def one_gather(arrays, axis, dims):
    flat = jnp.concatenate([a.reshape(-1) for a in arrays])
    lines, at, done = lax.all_gather(flat, axis), 0, []
    for a, dim in zip(arrays, dims):
        pieces = lines[:, at : at + a.size].reshape(-1, *a.shape)
        done.append(in_order(pieces, dim))
        at += a.size
    return tuple(done)


def gather_axes(x, axes, dim):
    filled = x
    for number in range(len(axes) - 1, -1, -1):
        filled = lax.all_gather(filled, axes[number], axis=dim, tiled=True)
    return filled


def cut_rows(length, count):
    unit = 8 if length >= 8 * count else 1
    return [length // unit * k // count * unit for k in range(1, count)]


def all_blocks(x, axes, sequence):
    pieces = x
    for k in sequence:
        pieces = lax.all_gather(pieces, axes[k])
    done = sequence[::-1]
    back = [done.index(k) for k in range(len(axes))]
    pieces = pieces.transpose(*back, *range(len(axes), pieces.ndim))
    return pieces.reshape(-1, *x.shape)


def gather_at_once(x, axes, dim):
    cut = max(range(max(1, x.ndim - 1)), key=lambda d: x.shape[d])
    count, done = len(axes), []
    for leading, piece in enumerate(jnp.split(x, cut_rows(x.shape[cut], count), axis=cut)):
        if piece.size:
            sequence = [(leading - k) % count for k in range(count)]
            done.append(all_blocks(piece, axes, sequence))
    return in_order(jnp.concatenate(done, axis=cut + 1), dim)


def worked_whole(x, axes, dim, apply):
    return apply(gather_at_once(x, axes, dim), jnp.int32(0))


def as_sent(x):
    return jax.tree.map(lambda a: a.astype(jnp.bfloat16) if a.dtype == jnp.float32 else a, x)


def passed_along(x, axis, by):
    length = lax.axis_size(axis)
    pairs = [(i, i + by) for i in range(length) if 0 <= i + by < length]
    return lax.ppermute(x, axis, pairs)


def neutral_like(x, identity):
    return jax.tree.map(
        lambda a, e: jnp.broadcast_to(jnp.asarray(e, a.dtype), a.shape), x, identity
    )


def entering(x, axes, combine, identity, reverse):
    before = start = neutral_like(x, identity)
    subtotal = x
    for axis in reversed(axes):
        length, here = lax.axis_size(axis), lax.axis_index(axis)
        pieces = jax.tree.map(lambda part: lax.all_gather(part, axis), subtotal)
        inside, subtotal = start, start
        for k in reversed(range(length)) if reverse else range(length):
            passed = k > here if reverse else k < here
            subtotal = combine(subtotal, jax.tree.map(lambda part: part[k], pieces))
            inside = jax.tree.map(lambda new, old: jnp.where(passed, new, old), subtotal, inside)
        before = combine(inside, before)
    return before


def own_rows(term, span, axes):
    subtotal = term(jnp.int32(0), span * lax.axis_size(axes)).astype(jnp.bfloat16)
    for axis in axes:
        subtotal = lax.psum_scatter(subtotal, axis, scatter_dimension=0, tiled=True)
    return subtotal.astype(jnp.float32)


def unit_inverse(lower):
    size = lower.shape[-1]
    inverse = jnp.eye(size, dtype=jnp.float32) - lower
    power = jnp.matmul(lower, lower, precision=highest)
    span = 2
    while span < size:
        inverse = inverse + jnp.matmul(inverse, power, precision=highest)
        power = jnp.matmul(power, power, precision=highest)
        span = span * 2
    return inverse


def make_terms(query, keys, values, beta, rate_col):
    size = query.shape[-2]
    steps = jnp.arange(1, size + 1).astype(jnp.float32)
    cumulative = -rate_col * steps
    lower_mask = jnp.tril(jnp.ones((size, size), bool))
    strict_mask = jnp.tril(jnp.ones((size, size), bool), -1)
    decay = jnp.where(lower_mask, jnp.exp(cumulative[..., :, None] - cumulative[..., None, :]), 0.0)
    weighted = keys * beta[..., None]
    lower = jnp.where(
        strict_mask,
        jnp.einsum("...cd,...sd->...cs", weighted, keys, precision=highest) * decay,
        0.0,
    )
    inverse = unit_inverse(lower)
    update = jnp.einsum("...cs,...sv->...cv", inverse, values * beta[..., None], precision=highest)
    erase = jnp.einsum(
        "...cs,...sd->...cd", inverse, weighted * jnp.exp(cumulative)[..., None], precision=highest
    )
    scores = jnp.einsum("...cd,...sd->...cs", query, keys, precision=highest) * decay
    query_decayed = query * jnp.exp(cumulative)[..., None]
    final = cumulative[..., -1:]
    keys_decayed = keys * jnp.exp(final - cumulative)[..., None]
    return (query_decayed, keys_decayed, update, erase, scores, jnp.exp(final))


def apply_block(state, terms):
    query_decayed, keys_decayed, update, erase, scores, kept = terms
    fresh = update - jnp.einsum("...cd,...dv->...cv", erase, state, precision=highest)
    output = jnp.einsum("...cd,...dv->...cv", query_decayed, state, precision=highest)
    output = output + jnp.einsum("...cs,...sv->...cv", scores, fresh, precision=highest)
    state = state * kept[..., None] + jnp.einsum(
        "...cd,...cv->...dv", keys_decayed, fresh, precision=highest
    )
    return (state, output)


def causal_conv(pre, conv_taps, history):
    width = conv_taps.shape[0]
    extended = jnp.concatenate([history, pre], axis=0).astype(jnp.float32)
    length = pre.shape[0]
    total = jnp.zeros(pre.shape, jnp.float32)
    for tap in range(width):
        total = total + extended[tap : tap + length] * conv_taps[tap].astype(jnp.float32)
    return total


def rms_scale(values_in, gain):
    values = values_in.astype(jnp.float32)
    scaled = values * lax.rsqrt(jnp.mean(values * values, axis=-1, keepdims=True) + epsilon)
    return (scaled * gain).astype(jnp.bfloat16)


def l2_normalize(array):
    return array * lax.rsqrt(jnp.sum(array * array, axis=-1, keepdims=True) + epsilon)


def finish(outputs, out_gain, gate_pre):
    normed = (
        outputs
        * lax.rsqrt(jnp.mean(outputs * outputs, axis=-1, keepdims=True) + out_epsilon)
        * out_gain
    )
    gate = jax.nn.silu(gate_pre.astype(jnp.float32)).reshape(outputs.shape)
    return (normed * gate).astype(jnp.bfloat16).reshape(outputs.shape[0], outputs.shape[1], -1)


def compose(earlier, later):
    first_map, first_shift = earlier
    second_map, second_shift = later
    joined_map = jnp.einsum("shde,shef->shdf", second_map, first_map, precision=highest)
    joined_shift = (
        jnp.einsum("shde,shev->shdv", second_map, first_shift, precision=highest) + second_shift
    )
    return (joined_map, joined_shift)


def shards(
    tokens,
    in_gain,
    w_query,
    w_key,
    w_value,
    w_gate,
    w_beta,
    conv_query,
    conv_key,
    conv_value,
    decay_rate,
    out_gain,
    w_out,
):
    rows = tokens.shape[0]
    seq_count = tokens.shape[1]
    width = tokens.shape[2]
    head_width = w_query.shape[1]
    local_heads = w_beta.shape[1]
    depth = head_width // local_heads
    normed = rms_scale(tokens, in_gain)
    full_query, full_key, full_value, full_gate, full_beta = one_gather(
        (w_query, w_key, w_value, w_gate, w_beta), SP, (0, 0, 0, 0, 0)
    )
    full_out = gather_axes(w_out, SP, 1)

    def project(piece, start):
        flat = piece.reshape(-1, width)
        parts = [
            jnp.dot(flat, weight, preferred_element_type=jnp.float32).astype(jnp.bfloat16)
            for weight in (full_query, full_key, full_value, full_gate, full_beta)
        ]
        return jnp.concatenate(parts, axis=1).reshape(piece.shape[0], seq_count, -1)

    projected = worked_whole(normed, TP, 0, project)
    span = projected.shape[0]
    mixed_pre = projected[:, :, : 3 * head_width]
    gate_pre = projected[:, :, 3 * head_width : 4 * head_width]
    beta_pre = projected[:, :, 4 * head_width :]
    taps = conv_query.shape[0]
    history = passed_along(as_sent(mixed_pre[span - taps + 1 :]), SP, 1)
    conv_taps = jnp.concatenate([conv_query, conv_key, conv_value], axis=1)
    convolved = jax.nn.silu(causal_conv(mixed_pre, conv_taps, history))

    def split_heads(array):
        return array.reshape(span, seq_count, local_heads, depth)

    query = l2_normalize(split_heads(convolved[:, :, :head_width])) * depth ** (-0.5)
    keys = l2_normalize(split_heads(convolved[:, :, head_width : 2 * head_width]))
    values = split_heads(convolved[:, :, 2 * head_width :])
    total_tokens = span * lax.axis_size(SP)
    beta = jax.nn.sigmoid(beta_pre.astype(jnp.float32) + math.log(depth / (4.0 * total_tokens)))
    rate_col = (decay_rate / total_tokens)[:, None]
    blocks = span // BLOCK

    def to_blocks(array):
        return jnp.moveaxis(array.reshape(blocks, BLOCK, seq_count, local_heads, depth), 1, 3)

    beta_blocks = jnp.moveaxis(beta.reshape(blocks, BLOCK, seq_count, local_heads), 1, 3)
    query_decayed, keys_decayed, update, erase, scores, kept = make_terms(
        to_blocks(query), to_blocks(keys), to_blocks(values), beta_blocks, rate_col
    )
    identity = jnp.broadcast_to(
        jnp.eye(depth, dtype=jnp.float32), (seq_count, local_heads, depth, depth)
    )
    zeros = jnp.zeros((seq_count, local_heads, depth, depth), jnp.float32)
    transfer = identity
    offset = zeros
    local_outputs = []
    readouts = []
    for index in range(blocks):
        block_terms = (
            query_decayed[index],
            keys_decayed[index],
            update[index],
            erase[index],
            scores[index],
            kept,
        )
        offset_next, output = apply_block(offset, block_terms)
        local_outputs.append(output)
        reach = query_decayed[index] - jnp.einsum(
            "shct,shtd->shcd", scores[index], erase[index], precision=highest
        )
        readouts.append(jnp.einsum("shcd,shde->shce", reach, transfer, precision=highest))
        erased = jnp.einsum("shcd,shde->shce", erase[index], transfer, precision=highest)
        transfer = transfer * kept[..., None] - jnp.einsum(
            "shcd,shce->shde", keys_decayed[index], erased, precision=highest
        )
        offset = offset_next
    prefix = entering((as_sent(transfer), as_sent(offset)), SP, compose, (identity, zeros), False)
    incoming = prefix[1]
    outputs = jnp.stack(local_outputs) + jnp.einsum(
        "nshcd,shdv->nshcv", jnp.stack(readouts), incoming, precision=highest
    )
    outputs = jnp.moveaxis(outputs, 3, 1).reshape(span, seq_count, local_heads, depth)
    gated = finish(outputs, out_gain, gate_pre)

    def head_term(start, count_rows):
        block = lax.dynamic_slice_in_dim(gated, start, count_rows, 0)
        flat = block.reshape(-1, head_width)
        return jnp.dot(flat, full_out, preferred_element_type=jnp.float32).reshape(
            count_rows, seq_count, -1
        )

    summed = own_rows(head_term, rows, TP)
    return summed.astype(jnp.bfloat16)


def solution(mesh):
    finer = Mesh(mesh.devices.reshape(16, 4, 4, 2), ("sp_0", "sp_1", "tp_0", "tp_1"))
    return jax.shard_map(
        shards,
        mesh=finer,
        in_specs=(
            P(SP_TP, None, None),
            P(),
            P(SP, TP),
            P(SP, TP),
            P(SP, TP),
            P(SP, TP),
            P(SP, TP),
            P(None, TP),
            P(None, TP),
            P(None, TP),
            P(TP),
            P(),
            P(TP, SP),
        ),
        out_specs=P(SP_TP, None, None),
        check_vma=False,
    )
```

profile of v0, /device:TPU:1, one launch (start us, length us, event | category | flops | bytes accessed | tf_op | source)
XLA Modules:
  0.0 561.1 jit_solution(10700707237145528193)
XLA Ops:
  7.3 1.3 dynamic-slice
  15.7 8.3 %all-gather.2 = bf16[12,4,1024]{2,1,0:T(4,128)(2,1)S(1)} all-gather(bf16[6,4,1024]{2,1,0:T(4,128)(2,1)S(1)} %get-tuple-element.19), channel_id=4, replica_groups=mesh['sp_0'=16,'sp_1'=4,'tp_0'=4,'tp_1'=2] {'tp_1'}, dimensions={0}, use_global_device_ids=true | all-gather | bytes 147456 | tf_op jit(solution)/shard_map/all_gather | solution.py:51
  24.0 9.2 %all-gather = bf16[24,4,1024]{2,1,0:T(4,128)(2,1)S(1)} all-gather(bf16[6,4,1024]{2,1,0:T(4,128)(2,1)S(1)} %get-tuple-element.18), channel_id=2, replica_groups=mesh['sp_0'=16,'sp_1'=4,'tp_0'=4,'tp_1'=2] {'tp_0'}, dimensions={0}, use_global_device_ids=true | all-gather | bytes 245760 | tf_op jit(solution)/shard_map/all_gather | solution.py:51
  33.3 5.0 all-gather.1
  38.4 10.2 %all-gather.3 = bf16[8,6,4,1024]{3,2,1,0:T(4,128)(2,1)S(1)} all-gather(bf16[2,6,4,1024]{3,2,1,0:T(4,128)(2,1)S(1)} %bitcast.294), channel_id=5, replica_groups=mesh['sp_0'=16,'sp_1'=4,'tp_0'=4,'tp_1'=2] {'tp_0'}, dimensions={0}, use_global_device_ids=true | all-gather | bytes 491520 | tf_op jit(solution)/shard_map/all_gather | solution.py:51
  50.3 237.1 %all-reduce.5.cloned.1.call-done = bf16[525312]{0:T(1024)(128)(2,1)} async-done(((bf16[525312]{0:T(1024)(128)(2,1)}), bf16[525312]{0:T(1024)(128)(2,1)}) %all-reduce.5.cloned.1.call-update) | async-done | bytes 1050640
  287.3 2.6 reshape.857
  292.2 1.8 collective-permute-start
  298.4 10.4 %all-gather.5 = bf16[16,128,128]{2,1,0:T(8,128)(2,1)S(1)} all-gather(bf16[4,128,128]{2,1,0:T(8,128)(2,1)S(1)} %fusion.1), channel_id=7, replica_groups=mesh['sp_0'=16,'sp_1'=4,'tp_0'=4,'tp_1'=2] {'sp_1'}, dimensions={0}, use_global_device_ids=true | all-gather | bytes 655360 | tf_op jit(solution)/shard_map/all_gather | solution.py:93
  312.3 11.3 %all-gather.7 = bf16[16,128,128]{2,1,0:T(8,128)(2,1)S(1)} all-gather(bf16[4,128,128]{2,1,0:T(8,128)(2,1)S(1)} %fusion.2), channel_id=9, replica_groups=mesh['sp_0'=16,'sp_1'=4,'tp_0'=4,'tp_1'=2] {'sp_1'}, dimensions={0}, use_global_device_ids=true | all-gather | bytes 655360 | tf_op jit(solution)/shard_map/all_gather | solution.py:93
  327.9 9.3 %all_gather.78 = bf16[128,64]{0,1:T(8,128)(2,1)S(1)} all-gather(bf16[128,16]{0,1:T(8,128)(2,1)S(1)} %copy-done.18), channel_id=1, replica_groups=mesh['sp_0'=16,'sp_1'=4,'tp_0'=4,'tp_1'=2] {'sp_1'}, dimensions={1}, use_global_device_ids=true | all-gather | bytes 20480 | tf_op jit(solution)/shard_map/all_gather | solution.py:39
  337.2 27.0 %all_gather.79 = bf16[128,1024]{0,1:T(8,128)(2,1)S(1)} all-gather(bf16[128,64]{0,1:T(8,128)(2,1)S(1)} %all_gather.78), channel_id=1, replica_groups=mesh['sp_0'=16,'sp_1'=4,'tp_0'=4,'tp_1'=2] {'sp_0'}, dimensions={1}, use_global_device_ids=true | all-gather | bytes 278528 | tf_op jit(solution)/shard_map/all_gather | solution.py:39
  369.0 18.6 %all-gather.12.cloned.1.call-done = bf16[64,128,128]{2,1,0:T(8,128)(2,1)} async-done(((bf16[4,128,128]{2,1,0:T(8,128)(2,1)}), bf16[64,128,128]{2,1,0:T(8,128)(2,1)}) %all-gather.12.cloned.1.call-update) | async-done | bytes 2097168 | tf_op jit(solution)/shard_map/all_gather | solution.py:93
  387.6 71.7 %all-gather.14.cloned.1.call-done = bf16[64,128,128]{2,1,0:T(8,128)(2,1)} async-done(((bf16[4,128,128]{2,1,0:T(8,128)(2,1)}), bf16[64,128,128]{2,1,0:T(8,128)(2,1)}) %all-gather.14.cloned.1.call-update) | async-done | bytes 2097168 | tf_op jit(solution)/shard_map/all_gather | solution.py:93
  459.3 1.3 convolution_add_fusion.26
  460.6 1.1 convolution_add_fusion.21
  461.7 1.1 convolution_add_fusion.20
  468.8 1.2 fusion.11
  470.1 1.3 multiply_reduce_fusion
  473.0 34.6 %reduce-scatter.4.cloned.1.call-done = bf16[24,4096]{1,0:T(8,128)(2,1)} async-done(((bf16[96,4096]{1,0:T(8,128)(2,1)}), bf16[24,4096]{1,0:T(8,128)(2,1)}) %reduce-scatter.4.cloned.1.call-update) | async-done | bytes 196624
  507.6 1.7 reshape.954
  509.4 1.3 dynamic-slice.1
  511.3 41.7 %all-reduce.7.cloned.1.call-done = bf16[24,4,1024]{2,1,0:T(4,128)(2,1)} async-done(((bf16[24,4,1024]{2,1,0:T(4,128)(2,1)}), bf16[24,4,1024]{2,1,0:T(4,128)(2,1)}) %all-reduce.7.cloned.1.call-update) | async-done | bytes 196624
  553.0 1.6 constant_dynamic-slice_fusion
  (172 shorter events, 33.7 us)
Async XLA Ops:
  6.5 8.8 %copy-start.21 = (bf16[4,128]{1,0:T(4,128)(2,1)S(1)}, bf16[4,128]{1,0:T(4,128)(2,1)}, u32[]{:S(2)}) copy-start(bf16[4,128]{1,0:T(4,128)(2,1)} %param.20) | copy-start | bytes 3076
  6.5 8.8 %copy-start.9 = (bf16[12,4,1024]{2,1,0:T(4,128)(2,1)S(1)}, bf16[12,4,1024]{2,1,0:T(4,128)(2,1)}, u32[]{:S(2)}) copy-start(bf16[12,4,1024]{2,1,0:T(4,128)(2,1)} %param.13) | copy-start | bytes 294916
  6.5 9.0 %copy-start.17 = (f32[1024]{0:T(1024)S(1)}, f32[1024]{0:T(1024)}, u32[]{:S(2)}) copy-start(f32[1024]{0:T(1024)} %param.14) | copy-start | bytes 12292
  6.5 280.8 %all-reduce.5.cloned.1.call-start = ((), (), s32[]{:S(2)}) async-start(), calls=%async_computation.3 | async-start | bytes 2101248
  12.0 36.7 %copy-start.22 = (bf16[4,128]{1,0:T(4,128)(2,1)S(1)}, bf16[4,128]{1,0:T(4,128)(2,1)}, u32[]{:S(2)}) copy-start(bf16[4,128]{1,0:T(4,128)(2,1)} %param.21) | copy-start | bytes 3076
  12.0 36.7 %copy-start.23 = (bf16[4,128]{1,0:T(4,128)(2,1)S(1)}, bf16[4,128]{1,0:T(4,128)(2,1)}, u32[]{:S(2)}) copy-start(bf16[4,128]{1,0:T(4,128)(2,1)} %param.22) | copy-start | bytes 3076
  13.5 374.1 %all-gather.12.cloned.1.call-start = ((), (), s32[]{:S(2)}) async-start(), calls=%async_computation.1 | async-start | bytes 2228224 | tf_op jit(solution)/shard_map/all_gather | solution.py:93
  14.2 283.1 %copy-start.19 = (f32[32]{0:T(128)}, f32[32]{0:T(128)S(1)}, u32[]{:S(2)}) copy-start(f32[32]{0:T(128)S(1)} %fusion.124) | copy-start | bytes 388
  50.0 258.8 %copy-start.14 = (bf16[128,128]{1,0:T(8,128)(2,1)}, bf16[128,128]{1,0:T(8,128)(2,1)S(1)}, u32[]{:S(2)}) copy-start(bf16[128,128]{1,0:T(8,128)(2,1)S(1)} %fusion.110) | copy-start | bytes 98308
  50.0 247.5 %copy-start.10 = (bf16[128,128]{1,0:T(8,128)(2,1)}, bf16[128,128]{1,0:T(8,128)(2,1)S(1)}, u32[]{:S(2)}) copy-start(bf16[128,128]{1,0:T(8,128)(2,1)S(1)} %fusion.107) | copy-start | bytes 98308
  292.2 2.6 collective-permute-start
  309.0 1.9 copy-start.4
  310.2 149.0 %all-gather.14.cloned.1.call-start = ((), (), s32[]{:S(2)}) async-start(), calls=%async_computation.2 | async-start | bytes 2228224 | tf_op jit(solution)/shard_map/all_gather | solution.py:93
  312.3 15.6 %copy-start.18 = (bf16[128,16]{0,1:T(8,128)(2,1)S(1)}, bf16[128,16]{0,1:T(8,128)(2,1)}, u32[]{:S(2)}) copy-start(bf16[128,16]{0,1:T(8,128)(2,1)} %param.25) | copy-start | bytes 12292
  324.4 40.3 %copy-start.20 = (f32[32]{0:T(128)S(1)}, f32[32]{0:T(128)}, u32[]{:S(2)}) copy-start(f32[32]{0:T(128)} %copy-done.19) | copy-start | bytes 388
  327.8 38.4 %copy-start.13 = (bf16[4,32,128]{2,1,0:T(8,128)(2,1)S(1)}, bf16[4,32,128]{2,1,0:T(8,128)(2,1)}, u32[]{:S(2)}) copy-start(bf16[4,32,128]{2,1,0:T(8,128)(2,1)} %copy-done.12) | copy-start | bytes 98308
  327.8 179.8 %reduce-scatter.4.cloned.1.call-start = ((), (), s32[]{:S(2)}) async-start(), calls=%async_computation.4 | async-start | bytes 983040
  337.2 29.8 %copy-start.11 = (bf16[128,128]{1,0:T(8,128)(2,1)S(1)}, bf16[128,128]{1,0:T(8,128)(2,1)}, u32[]{:S(2)}) copy-start(bf16[128,128]{1,0:T(8,128)(2,1)} %copy-done.10) | copy-start | bytes 98308
  387.6 75.3 %copy-start = (bf16[64,128,128]{2,1,0:T(8,128)(2,1)S(1)}, bf16[64,128,128]{2,1,0:T(8,128)(2,1)}, u32[]{:S(2)}) copy-start(bf16[64,128,128]{2,1,0:T(8,128)(2,1)} %all-gather.12.cloned.1.call-done) | copy-start | bytes 6291460
  459.3 6.8 %copy-start.2 = (bf16[64,128,128]{2,1,0:T(8,128)(2,1)S(1)}, bf16[64,128,128]{2,1,0:T(8,128)(2,1)}, u32[]{:S(2)}) copy-start(bf16[64,128,128]{2,1,0:T(8,128)(2,1)} %all-gather.14.cloned.1.call-done) | copy-start | bytes 6291460
  467.8 2.2 copy-start.7
  467.8 2.2 copy-start.16
  468.8 2.7 copy-start.24
  472.9 80.0 %all-reduce.7.cloned.1.call-start = ((), (), s32[]{:S(2)}) async-start(), calls=%async_computation.5 | async-start | bytes 393216
  (7 other events, 6.5 us)
Sparse Core Ops, SparseCore 0:
  13.6 273.7 all-reduce.4
  310.4 77.1 all-gather.11
  389.7 69.5 all-gather.13
  473.0 34.5 reduce-scatter.3
  510.3 42.5 all-reduce.6
where the time goes:
time: 562 us; the launch traced here: 561 us
  waiting for transfers between devices  404 us (72%)
  blocking collectives  90.7 us (16%)
  matrix products  26.4 us (5%)
  local copies, waits for them, and re-layouts  18.4 us (3%)
  between operations  16.6 us (3%)
    unnamed x8, waiting for transfers between devices  313 us
    all_gather x2, waiting for transfers between devices, entering(): pieces = jax.tree.map(lambda part: lax.all_gather(part, axis), subtotal)  90.3 us
    all_gather x2, blocking collectives, gather_axes(): filled = lax.all_gather(filled, axes[number], axis=dim, tiled=True)  36.2 us
    all_gather x4, blocking collectives, all_blocks(): pieces = lax.all_gather(pieces, axes[k])  32.8 us
    all_gather x2, blocking collectives, entering(): pieces = jax.tree.map(lambda part: lax.all_gather(part, axis), subtotal)  21.7 us
    dot_general x21, matrix products, compose(): jnp.einsum('shde,shev->shdv', second_map, first_shift, precision=highest)  13.4 us
    unnamed x64, local copies, waits for them, and re-layouts  11.4 us
  transfers between devices with their start and end apart: 6, of which 6 were waited for; matrix products, arithmetic and copies ran while one was open for 2% of the time, Pallas kernels for 0%

commit v1 on v0

v1 whole, which is shorter than its diff:
```python
import math

import jax
import jax.numpy as jnp
from jax import lax
from jax.experimental import pallas as pl
from jax.experimental.pallas import tpu as pltpu
from jax.sharding import PartitionSpec as P

MESH = pl.DeviceIdType.MESH
F32 = jnp.float32
BF16 = jnp.bfloat16

Z, Y, X, C = 16, 4, 4, 2
TP = X * C
ROWS = 16
PAD = 4
TOK = ROWS - PAD
PLANE = Y * TP
CHUNK = 128
CHUNKS = PLANE * ROWS // CHUNK
CHUNK_TOKENS = CHUNK // ROWS * TOK
TOKENS = 6144
D = 1024
DK = 128
WIDE = 5 * DK

epsilon = 1e-06
out_epsilon = 1e-10


def place():
    sp, tp = lax.axis_index("sp"), lax.axis_index("tp")
    return sp // Y, sp % Y, tp // C, tp % C


def at(z, y, x, c):
    return ((z + Z) % Z * Y + (y + Y) % Y, (x + X) % X * C + (c + C) % C)


def meet(peers):
    barrier = pltpu.get_barrier_semaphore()
    for peer in peers:
        pl.semaphore_signal(barrier, inc=1, device_id=peer, device_id_type=MESH)
    pl.semaphore_wait(barrier, len(peers))


def remote(src, dst, send, recv, peer):
    return pltpu.make_async_remote_copy(
        src_ref=src, dst_ref=dst, send_sem=send, recv_sem=recv, device_id=peer, device_id_type=MESH
    )


NEAR = (-1, 1, 2)


def gather_kernel(nrm, wblk, wob, xf, wf, wo, local, s_tok, r_tok, s_w, r_w, s_o, r_o):
    z, y, x, c = place()
    tp = x * C + c
    zh, zl = z // 4, z % 4
    meet(
        [at(z + k, y, x, c) for k in (-1, 1, -2, 2, 4, 8, 12)]
        + [at(z, y + k, x, c) for k in (1, 2, 3)]
        + [at(z, y, x + k, c) for k in (1, 2, 3)]
        + [at(z, y, x, c + 1)]
    )
    sent = []

    def go(copy):
        copy.start()
        sent.append(copy)
        return copy

    def block(ys, k):
        return xf.at[1 + (y + ys + Y) % Y * TP + (x + k + X) % X * C + c]

    own_x = xf.at[1 + y * TP + tp]
    w1 = [go(remote(wblk, wf.at[zh, zl, y], s_w.at[k], r_w.at[k], at(z + 4 * k + 4, y, x, c))) for k in range(3)]
    o1 = [go(remote(wob, wo.at[zh, zl, y], s_o.at[k], r_o.at[k], at(z + 4 * k + 4, y, x, c))) for k in range(3)]
    t1 = [
        go(remote(nrm.at[(y + k + 1) % Y], own_x, s_tok.at[k], r_tok.at[k], at(z, y + k + 1, x, c)))
        for k in range(3)
    ]
    t2, t3 = {}, {}

    def pass_x(ys, src):
        for k in range(3):
            i = 3 + ys * 3 + k
            t2[ys, k] = go(remote(src, block(-ys, 0), s_tok.at[i], r_tok.at[i], at(z, y, x + k + 1, c)))

    def pass_core(ys, k, src):
        i = 15 + ys * 4 + k
        t3[ys, k] = go(remote(src, block(-ys, -k), s_tok.at[i], r_tok.at[i], at(z, y, x, c + 1)))

    pass_x(0, nrm.at[y])
    pass_core(0, 0, nrm.at[y])
    mine = [
        pltpu.make_async_copy(wblk, wf.at[zh, zl, y], local.at[0]),
        pltpu.make_async_copy(wob, wo.at[zh, zl, y], local.at[1]),
        pltpu.make_async_copy(nrm.at[y], own_x, local.at[2]),
    ]
    for copy in mine:
        copy.start()
    for k in range(3):
        t1[k].wait_recv()
        pass_x(k + 1, block(-k - 1, 0))
        pass_core(k + 1, 0, block(-k - 1, 0))
    for ys in range(4):
        for k in range(3):
            t2[ys, k].wait_recv()
            pass_core(ys, k + 1, block(-ys, -k - 1))

    w3 = {}

    def pass_y(r, zr):
        for k in range(3):
            i = 6 + 3 * r + k
            part = wf.at[:, zr, y]
            w3[r, k] = go(remote(part, part, s_w.at[i], r_w.at[i], at(z, y + k + 1, x, c)))

    mine[0].wait()
    mine[1].wait()
    for copy in w1:
        copy.wait_recv()
    w2 = []
    for k, off in enumerate(NEAR):
        part = wf.at[:, zl, y]
        w2.append(go(remote(part, part, s_w.at[3 + k], r_w.at[3 + k], at(z + off, y, x, c))))
    pass_y(0, zl)
    for copy in o1:
        copy.wait_recv()
    o2 = []
    for k, off in enumerate(NEAR):
        part = wo.at[:, zl, y]
        o2.append(go(remote(part, part, s_o.at[3 + k], r_o.at[3 + k], at(z + off, y, x, c))))
    for k, off in enumerate(NEAR):
        w2[k].wait_recv()
        pass_y(k + 1, (z - off + Z) % 4)
    for copy in o2:
        copy.wait_recv()
    o3 = []
    for k in range(3):
        part = wo.at[:, :, y]
        o3.append(go(remote(part, part, s_o.at[6 + k], r_o.at[6 + k], at(z, y + k + 1, x, c))))

    mine[2].wait()
    for ys in range(4):
        for k in range(4):
            t3[ys, k].wait_recv()
    history = go(remote(xf.at[PLANE], xf.at[0], s_tok.at[31], r_tok.at[31], at(z + 1, y, x, c)))
    for copy in list(w3.values()) + o3 + [history]:
        copy.wait_recv()
    for copy in sent:
        copy.wait_send()


def gather(nrm, wblk, wob):
    vmem = pl.BlockSpec(memory_space=pltpu.VMEM)
    dma = pltpu.SemaphoreType.DMA
    return pl.pallas_call(
        gather_kernel,
        out_shape=(
            jax.ShapeDtypeStruct((PLANE + 1, ROWS, D), BF16),
            jax.ShapeDtypeStruct((4, 4, Y, 16, WIDE), BF16),
            jax.ShapeDtypeStruct((4, 4, Y, 16, DK), BF16),
        ),
        in_specs=[vmem] * 3,
        out_specs=(vmem,) * 3,
        scratch_shapes=[dma((3,)), dma((32,)), dma((32,)), dma((18,)), dma((18,)), dma((9,)), dma((9,))],
        compiler_params=pltpu.CompilerParams(collective_id=1, has_side_effects=True),
        name="gather",
    )(nrm, wblk, wob)


def mm(a, b, dims=((1,), (0,))):
    return lax.dot_general(a.astype(BF16), b.astype(BF16), (dims, ((), ())), preferred_element_type=F32)


def sigmoid(v):
    return 1.0 / (1.0 + jnp.exp(-v))


def local_kernel(rate, x, w, taps, maps, reach_out, local_out, gate_out, ext):
    pre = mm(x[...].reshape((PLANE + 1) * ROWS, D), w[...]).astype(BF16).astype(F32)
    total = PLANE * ROWS
    full = total + ROWS
    first = jnp.where(lax.axis_index("sp") // Y == 0, 0.0, 1.0).astype(F32)
    ext[...] = pre[:, : 3 * DK]
    ext[0:ROWS, :] = pre[:ROWS, : 3 * DK] * first
    gate_pre = pre[ROWS:, 3 * DK : 4 * DK]
    gate_out[...] = gate_pre * sigmoid(gate_pre)
    beta_pre = pre[ROWS:, 4 * DK : 4 * DK + 1]
    inner = lax.broadcasted_iota(jnp.int32, (total, 3 * DK), 0) % ROWS
    fixed = jnp.where(inner < PAD, ext[ROWS - PAD : full - PAD, :], ext[ROWS:full, :])
    ext[ROWS:full, :] = fixed
    conv = ext[ROWS:full, :] * taps[3:4, :]
    for k in range(1, 4):
        conv = conv + ext[ROWS - k : full - k, :] * taps[3 - k : 4 - k, :]
    conv = conv * sigmoid(conv)
    row = lax.broadcasted_iota(jnp.int32, (total, 1), 0)
    real = (row % ROWS >= PAD).astype(F32)
    q, k, v = conv[:, :DK], conv[:, DK : 2 * DK], conv[:, 2 * DK :]
    q = q * (lax.rsqrt(jnp.sum(q * q, axis=1, keepdims=True) + epsilon) * DK**-0.5)
    k = k * (lax.rsqrt(jnp.sum(k * k, axis=1, keepdims=True) + epsilon) * real)
    beta = sigmoid(beta_pre + math.log(DK / (4.0 * TOKENS))) * real

    lam = rate[0, 0] / TOKENS
    steps = lambda r: (r // ROWS * TOK + jnp.maximum(r % ROWS - (PAD - 1), 0)).astype(F32)
    ri = lax.broadcasted_iota(jnp.int32, (CHUNK, CHUNK), 0)
    ci = lax.broadcasted_iota(jnp.int32, (CHUNK, CHUNK), 1)
    decay = jnp.where(ri >= ci, jnp.exp(-lam * (steps(ri) - steps(ci))), 0.0)
    strict = jnp.where(ri > ci, decay, 0.0)
    in32 = ri // 32 == ci // 32
    in64 = ri // 64 == ci // 64
    eye = (ri == ci).astype(F32)
    here = steps(lax.broadcasted_iota(jnp.int32, (CHUNK, 1), 0))
    fall = jnp.exp(-lam * here)
    rest = jnp.exp(-lam * (CHUNK_TOKENS - here))
    kept = jnp.exp(jnp.full((1, 1), -1.0, F32) * lam * CHUNK_TOKENS)

    n = range(CHUNKS)
    cut = lambda a: [a[CHUNK * i : CHUNK * (i + 1)] for i in n]
    qs, ks, vs, bs = cut(q), cut(k), cut(v), cut(beta)
    ws = [ks[i] * bs[i] for i in n]
    both = [mm(jnp.concatenate([ws[i], qs[i]], axis=0), ks[i], ((1,), (1,))) for i in n]
    lower = [both[i][:CHUNK] * strict for i in n]
    scores = [both[i][CHUNK:] * decay for i in n]
    diag = [jnp.where(in32, lower[i], 0.0) for i in n]
    inverse = [eye - diag[i] for i in n]
    power = [mm(diag[i], diag[i]) for i in n]
    for step in range(4):
        inverse = [inverse[i] + mm(inverse[i], power[i]) for i in n]
        if step < 3:
            power = [mm(power[i], power[i]) for i in n]
    for inside, outside in ((in64, in32), (None, in64)):
        part = []
        for i in n:
            side = jnp.where(outside, 0.0, lower[i])
            part.append(side if inside is None else jnp.where(inside, side, 0.0))
        part = [mm(part[i], inverse[i]) for i in n]
        inverse = [inverse[i] - mm(inverse[i], part[i]) for i in n]
    pair = [mm(inverse[i], jnp.concatenate([ws[i] * fall, vs[i] * bs[i]], axis=1)) for i in n]
    read = [mm(scores[i], pair[i]) for i in n]
    grow = [mm(ks[i] * rest, pair[i], ((0,), (0,))) for i in n]
    reach = [qs[i] * fall - read[i][:, :DK] for i in n]
    erase = [kept * eye - grow[i][:, :DK] for i in n]
    shift = [grow[i][:, DK:] for i in n]
    state = None
    for i in n:
        out = slice(CHUNK * i, CHUNK * (i + 1))
        if state is None:
            reach_out[out, :] = reach[i].astype(BF16)
            local_out[out, :] = read[i][:, DK:]
            state = (erase[i], shift[i])
        else:
            joined = jnp.concatenate(state, axis=1)
            seen = mm(reach[i], joined)
            reach_out[out, :] = seen[:, :DK].astype(BF16)
            local_out[out, :] = seen[:, DK:] + read[i][:, DK:]
            after = mm(erase[i], joined)
            state = (after[:, :DK], after[:, DK:] + shift[i])
    maps[0] = state[0].astype(BF16)
    maps[1] = state[1].astype(BF16)


def local(rate, xf, wf, taps):
    vmem = pl.BlockSpec(memory_space=pltpu.VMEM)
    rows = PLANE * ROWS
    return pl.pallas_call(
        local_kernel,
        out_shape=(
            jax.ShapeDtypeStruct((2, DK, DK), BF16),
            jax.ShapeDtypeStruct((rows, DK), BF16),
            jax.ShapeDtypeStruct((rows, DK), F32),
            jax.ShapeDtypeStruct((rows, DK), F32),
        ),
        in_specs=[pl.BlockSpec(memory_space=pltpu.SMEM)] + [vmem] * 3,
        out_specs=(vmem,) * 4,
        scratch_shapes=[pltpu.VMEM((rows + ROWS, 3 * DK), F32)],
        name="local",
    )(rate, xf, wf, taps)


UP, DOWN = 8, 7


def finish_kernel(
    maps, reach, inner, gate, gain, woc, out, up, down, wall, gsend, gbuf, local, s_up, r_up, s_dn, r_dn, s_w, r_w, s_c, r_c, s_g, r_g
):
    z, y, x, c = place()
    tp = x * C + c
    others = [((z * Y + (y + dy) % Y), (tp + dt) % TP) for dy in range(Y) for dt in range(TP) if dy or dt]
    meet([at(z - 1, y, x, c), at(z + 1, y, x, c)] + others)
    sent = []

    def go(copy):
        copy.start()
        sent.append(copy)
        return copy

    ups, downs = {}, {}

    def send_up(d, p, src):
        i = 2 * d + p
        ups[d + 1, p] = go(remote(src, up.at[d, p], s_up.at[i], r_up.at[i], at(z + 1, y, x, c)))

    def send_down(d, p, src):
        i = 2 * d + p
        downs[d + 1, p] = go(remote(src, down.at[d, p], s_dn.at[i], r_dn.at[i], at(z - 1, y, x, c)))

    for p in range(2):
        send_up(0, p, maps.at[p])
        send_down(0, p, maps.at[p])

    def column(k):
        return wall.at[:, :, :, :, pl.ds(pl.multiple_of(((x - k + X) % X * C + c) * DK, DK), DK)]

    own = pltpu.make_async_copy(woc, column(0), local.at[0])
    own.start()
    wx = [go(remote(woc, column(0), s_w.at[k], r_w.at[k], at(z, y, x + k + 1, c))) for k in range(3)]
    wc = [go(remote(woc, column(0), s_c.at[0], r_c.at[0], at(z, y, x, c + 1)))]

    a_map = (
        lax.broadcasted_iota(jnp.int32, (DK, DK), 0) == lax.broadcasted_iota(jnp.int32, (DK, DK), 1)
    ).astype(F32)
    a_shift = jnp.zeros((DK, DK), F32)
    state = jnp.zeros((DK, DK), F32)
    for d in range(1, UP + 1):
        for p in range(2):
            ups[d, p].wait_recv()
            if d < UP:
                send_up(d, p, up.at[d - 1, p])
            if d <= DOWN:
                downs[d, p].wait_recv()
                if d < DOWN:
                    send_down(d, p, down.at[d - 1, p])
        there = d <= z
        new_shift = mm(a_map, up[d - 1, 1]) + a_shift
        new_map = mm(a_map, up[d - 1, 0])
        a_shift = jnp.where(there, new_shift, a_shift)
        a_map = jnp.where(there, new_map, a_map)
        if d <= DOWN:
            state = jnp.where(z + d >= Z, mm(down[d - 1, 0], state) + down[d - 1, 1].astype(F32), state)
    state = mm(a_map, state) + a_shift
    o = mm(reach[...], state) + inner[...]
    o = o * lax.rsqrt(jnp.mean(o * o, axis=1, keepdims=True) + out_epsilon) * gain[...] * gate[...]
    gsend[...] = o.astype(BF16).reshape(Y, TP, ROWS, DK)

    lane = pl.ds(pl.multiple_of(tp * DK, DK), DK)
    target = gbuf.at[y, :, lane]
    mine = pltpu.make_async_copy(gsend.at[y, tp], target, local.at[1])
    mine.start()
    gs = []
    for i, (sp, t) in enumerate(others):
        gs.append(go(remote(gsend.at[sp % Y, t], target, s_g.at[i], r_g.at[i], (sp, t))))

    own.wait()
    for k in range(3):
        wx[k].wait_recv()
        part = column(k + 1)
        wc.append(go(remote(part, part, s_c.at[k + 1], r_c.at[k + 1], at(z, y, x, c + 1))))
    for copy in wc:
        copy.wait_recv()
    mine.wait()
    for copy in gs:
        copy.wait_recv()
    full = lax.dot_general(
        gbuf[...].reshape(Y * ROWS, D),
        wall[...].reshape(D, D),
        (((1,), (1,)), ((), ())),
        preferred_element_type=F32,
    )
    out[...] = full.astype(BF16).reshape(Y, ROWS, D)
    for copy in sent:
        copy.wait_send()


def finish(maps, reach, inner, gate, gain, woc):
    vmem = pl.BlockSpec(memory_space=pltpu.VMEM)
    dma = pltpu.SemaphoreType.DMA
    return pl.pallas_call(
        finish_kernel,
        out_shape=jax.ShapeDtypeStruct((Y, ROWS, D), BF16),
        in_specs=[vmem] * 6,
        out_specs=vmem,
        scratch_shapes=[
            pltpu.VMEM((UP, 2, DK, DK), BF16),
            pltpu.VMEM((DOWN, 2, DK, DK), BF16),
            pltpu.VMEM((4, 4, Y, 16, D), BF16),
            pltpu.VMEM((Y, TP, ROWS, DK), BF16),
            pltpu.VMEM((Y, ROWS, D), BF16),
            dma((2,)),
            dma((2 * UP,)),
            dma((2 * UP,)),
            dma((2 * DOWN,)),
            dma((2 * DOWN,)),
            dma((3,)),
            dma((3,)),
            dma((4,)),
            dma((4,)),
            dma((PLANE - 1,)),
            dma((PLANE - 1,)),
        ],
        compiler_params=pltpu.CompilerParams(collective_id=2, has_side_effects=True),
        name="finish",
    )(maps, reach, inner, gate, gain, woc)


def rms_scale(values_in, gain):
    values = values_in.astype(F32)
    scaled = values * lax.rsqrt(jnp.mean(values * values, axis=-1, keepdims=True) + epsilon)
    return (scaled * gain).astype(BF16)


def shards(
    tokens, in_gain, w_query, w_key, w_value, w_gate, w_beta, conv_query, conv_key, conv_value, decay_rate, out_gain, w_out
):
    nrm = jnp.pad(jnp.swapaxes(rms_scale(tokens, in_gain), 0, 1), ((0, 0), (PAD, 0), (0, 0)))
    wblk = jnp.concatenate([w_query, w_key, w_value, w_gate, jnp.pad(w_beta, ((0, 0), (0, DK - 1)))], axis=1)
    taps = jnp.concatenate([conv_query, conv_key, conv_value], axis=1).astype(F32)
    xf, wf, wo = gather(nrm, wblk, w_out.T)
    maps, reach, inner, gate = local(decay_rate.reshape(1, 1), xf, wf.reshape(D, WIDE), taps)
    out = finish(maps, reach, inner, gate, out_gain.reshape(1, DK), wo)
    return jnp.swapaxes(out[:, PAD:], 0, 1)


def solution(mesh):
    both = ("sp", "tp")
    weight = P("sp", "tp")
    return jax.shard_map(
        shards,
        mesh=mesh,
        in_specs=(
            P(both, None, None),
            P(),
            weight,
            weight,
            weight,
            weight,
            weight,
            P(None, "tp"),
            P(None, "tp"),
            P(None, "tp"),
            P("tp"),
            P(),
            P("tp", "sp"),
        ),
        out_specs=P(both, None, None),
        check_vma=False,
    )
```

time: 562 us -> 105 us (0.19)
  waiting for transfers between devices: 404 us -> 0 us
  Pallas kernels: 0 us -> 94.8 us
  blocking collectives: 90.7 us -> 0 us
  matrix products: 26.4 us -> 0 us
  between operations: 16.6 us -> 0.69 us
  local copies, waits for them, and re-layouts: 18.4 us -> 5.89 us
    unnamed x8 -> x0, waiting for transfers between devices: 313 us -> none
    pallas_call x0 -> x3, Pallas kernels: none -> 94.8 us  [the longest x1 47.4 us: gather(): pl.pallas_call(gather_kernel, out_shape=(jax.ShapeDtypeStruct((PLANE + 1,...]
    all_gather x8 -> x0, blocking collectives: 90.7 us -> none  [the longest x2 36.2 us: gather_axes(): filled = lax.all_gather(filled, axes[number], axis=dim, tiled=True)]
    all_gather x2 -> x0, waiting for transfers between devices: 90.3 us -> none  [entering(): pieces = jax.tree.map(lambda part: lax.all_gather(part, axis), subtotal)]
    dot_general x61 -> x0, matrix products: 26.4 us -> none  [the longest x21 13.4 us: compose(): jnp.einsum('shde,shev->shdv', second_map, first_shift, precision=highest)]
    unnamed x64 -> x7, local copies, waits for them, and re-layouts: 11.4 us -> 3.53 us
  transfers between devices with their start and end apart: 6 -> 0, of which waited for: 6 -> 0; matrix products, arithmetic and copies ran while one was open for 2% -> 0% of each run, Pallas kernels for 0% -> 0%
where the time goes in v1:
time: 105 us
  Pallas kernels  94.8 us (90%)
  local copies, waits for them, and re-layouts  5.89 us (6%)
  other arithmetic  3.32 us (3%)
    pallas_call x1, Pallas kernels, gather(): pl.pallas_call(gather_kernel, out_shape=(jax.ShapeDtypeStruct((PLANE + 1,...  47.4 us
    pallas_call x1, Pallas kernels, finish(): pl.pallas_call(finish_kernel, out_shape=jax.ShapeDtypeStruct((Y, ROWS, D)...  41.1 us
    pallas_call x1, Pallas kernels, local(): pl.pallas_call(local_kernel, out_shape=(jax.ShapeDtypeStruct((2, DK, DK),...  6.36 us
    unnamed x7, local copies, waits for them, and re-layouts  3.53 us

profile of v1, /device:TPU:1, one launch (start us, length us, event | category | flops | bytes accessed | tf_op | source)
XLA Modules:
  0.0 104.7 jit_solution(4902869758391257750)
XLA Ops:
  0.7 1.0 fusion
  1.7 0.8 copy.15
  2.4 1.3 %maximum_convert_fusion.taps = f32[4,384]{1,0:T(4,128)} fusion(bf16[4,128]{1,0:T(4,128)(2,1)} %param.22, bf16[4,128]{1,0:T(4,128)(2,1)} %param.21, bf16[4,128]{1,0:T(4,128)(2,1)} %param.20), kind=kLoop, calls=%fused_computation.12 | loop fusion | flops 9216 | bytes 9216 | tf_op jit(solution)/shard_map/convert_element_type | solution.py:420
  3.7 0.7 constant_dynamic-update-slice_fusion.4
  4.4 0.7 constant_dynamic-update-slice_fusion.3
  5.1 0.7 constant_dynamic-update-slice_fusion.2
  5.8 0.7 constant_dynamic-update-slice_fusion.1
  6.5 0.0 copy-start
  6.5 1.0 fusion.3
  7.5 0.7 pad.8.nrm
  8.2 0.0 copy-done
  8.2 47.4 %gather.1 = (bf16[33,16,1024]{2,1,0:T(8,128)(2,1)}, bf16[4,4,4,16,640]{4,3,2,1,0:T(8,128)(2,1)}, bf16[4,4,4,16,128]{4,3,2,1,0:T(8,128)(2,1)}) custom-call(bf16[4,16,1024]{2,1,0:T(8,128)(2,1)} %pad.8.nrm, bf16[16,640]{1,0:T(8,128)(2,1)} %copy-done, bf16[16,128]{1,0:T(8,128)(2,1)} %bitcast.10), custom_call_target="tpu_custom_call" | custom-call | tf_op jit(solution)/shard_map/gather/pallas_call | solution.py:160
  55.6 6.4 %local.1 = (bf16[2,128,128]{2,1,0:T(8,128)(2,1)}, bf16[512,128]{1,0:T(8,128)(2,1)}, f32[512,128]{1,0:T(8,128)}, f32[512,128]{1,0:T(8,128)}) custom-call(f32[1,1]{1,0:T(1,128)} %bitcast.8.rate, bf16[33,16,1024]{2,1,0:T(8,128)(2,1)} %get-tuple-element.12.x, bf16[1024,640]{1,0:T(8,128)(2,1)} %bitcast.9, f32[4,384]{1,0:T(4,128)} %maximum_convert_fusion.taps), custom_call_target="tpu_custom_call" | custom-call | tf_op jit(solution)/shard_map/local/pallas_call | solution.py:269
  62.0 41.1 %finish.1 = bf16[4,16,1024]{2,1,0:T(8,128)(2,1)} custom-call(bf16[2,128,128]{2,1,0:T(8,128)(2,1)} %get-tuple-element.14.maps, bf16[512,128]{1,0:T(8,128)(2,1)} %get-tuple-element.15.reach, f32[512,128]{1,0:T(8,128)} %get-tuple-element.16.inner, f32[512,128]{1,0:T(8,128)} %get-tuple-element.17.gate, f32[1,128]{1,0:T(1,128)} %bitcast.11, ...), custom_call_target="tpu_custom_call" | custom-call | tf_op jit(solution)/shard_map/finish/pallas_call | solution.py:381
  103.0 0.9 slice_bitcast_fusion
  104.0 0.7 copy.16
  (2 shorter events, 0.0 us)
Async XLA Ops:
  6.5 1.7 %copy-start = (bf16[16,640]{1,0:T(8,128)(2,1)}, bf16[16,640]{1,0:T(8,128)(2,1)S(1)}, u32[]{:S(2)}) copy-start(bf16[16,640]{1,0:T(8,128)(2,1)S(1)} %constant_dynamic-update-slice_fusion.wblk) | copy-start | bytes 61444
